TPU v7x, 32 devices: a whole 2x2x4 slice. The times are simulated.
32 devices in a mesh: fs: 8 (over z, y), tp: 4 (over x, core).
Axes of the slice: x: 2, y: 2, z: 4, core: 2. Of those that a mesh axis runs over, the one named last changes fastest.
Arguments:
- prompt: bfloat16 [4096, 4096], P('fs'), may hold values from -6 to 6
- expert_ids: int32 [4096, 2], P('fs'), may hold values from 0 to 15, all different within a row; in each aligned block of 512 rows (0 to 511, 512 to 1023, ...) at most 96 rows name the same one
- group_weight: float32 [4096], P('fs'), may hold values from 0.25 to 1
- expert_share: float32 [4096, 2], P('fs'), may hold values from 0.1 to 1
- norm_gain: float32 [4096], P('fs'), may hold values from 0.1 to 1.9
- gate_train: float32 [16, 4096, 1024], P(None, 'fs', 'tp'), may hold values from -0.09375 to 0.09375
- up_train: float32 [16, 4096, 1024], P(None, 'fs', 'tp'), may hold values from -0.09375 to 0.09375
- down_train: float32 [16, 1024, 4096], P(None, 'fs', 'tp'), may hold values from -0.1875 to 0.1875
Outputs:
- mixed: bfloat16 [4096, 4096], P('fs', 'tp')
- gate_new: bfloat16 [16, 4096, 1024], P('fs', None, 'tp')
- up_new: bfloat16 [16, 4096, 1024], P('fs', None, 'tp')
- down_new: bfloat16 [16, 1024, 4096], P('fs', 'tp')
Inputs may be any that keep to these rules, and one draw needn't show every extreme that they name: `expert_ids`: each row names two different experts; within the rows of one index of fs no expert is named more than 96 times, a bound that some block reaches there.
All inputs are finite; a program needn't handle non-finite values.
Results may differ from a plain program's by a relative error of at most 0.0086.
Values may be sent and summed in bfloat16 or wider, within the bound.
No kernel may reach another device: no remote copies, remote signals or barrier semaphores. Data moves between devices by JAX's collectives and lax.ppermute only.
A program may use at most 128 MiB of HBM per device.

v0:
```python
import jax
import jax.numpy as jnp
from jax import lax
from jax.sharding import PartitionSpec as P

EPS = 1e-06


def on_device(
    prompt, expert_ids, group_weight, expert_share, norm_gain, gate_train, up_train, down_train
):
    gain_rows = norm_gain[None, :, None]
    gate_cast = (gate_train * gain_rows).astype(jnp.bfloat16)
    up_cast = (up_train * gain_rows).astype(jnp.bfloat16)
    gate_new, up_new = (
        lax.all_to_all(gate_cast, "fs", split_axis=0, concat_axis=1, tiled=True),
        lax.all_to_all(up_cast, "fs", split_axis=0, concat_axis=1, tiled=True),
    )
    down_cols = lax.all_to_all(
        down_train.astype(jnp.bfloat16), "fs", split_axis=0, concat_axis=1, tiled=True
    )
    down_new = lax.all_to_all(down_cols, "tp", split_axis=1, concat_axis=2, tiled=True)
    fs_count = lax.axis_size("fs")
    tp_count = lax.axis_size("tp")
    tokens, model_width = prompt.shape
    experts_all = gate_train.shape[0]
    local_experts = gate_new.shape[0]
    capacity = max(2, 3 * tokens // experts_all)
    widened = prompt.astype(jnp.float32)
    normed = (
        widened * lax.rsqrt(jnp.mean(widened * widened, axis=-1, keepdims=True) + EPS)
    ).astype(jnp.bfloat16)
    flat_ids = expert_ids.reshape(-1)
    onehot = (flat_ids[:, None] == jnp.arange(experts_all, dtype=jnp.int32)[None, :]).astype(
        jnp.int32
    )
    slot_rank = jnp.sum((jnp.cumsum(onehot, axis=0) - 1) * onehot, axis=1)
    targets = (flat_ids * capacity + slot_rank).reshape(tokens, 2)
    slot_ids = jnp.arange(experts_all * capacity, dtype=jnp.int32)
    picker = jnp.sum((targets[None, :, :] == slot_ids[:, None, None]).astype(jnp.bfloat16), axis=2)
    slice_width = model_width // tp_count
    own_columns = lax.dynamic_slice_in_dim(
        normed, lax.axis_index("tp") * slice_width, slice_width, 1
    )
    outgoing = jnp.dot(picker, own_columns, preferred_element_type=jnp.float32).astype(jnp.bfloat16)
    arrived = lax.all_to_all(
        outgoing.reshape(fs_count, local_experts, capacity, own_columns.shape[1]),
        "fs",
        split_axis=0,
        concat_axis=2,
        tiled=True,
    )[0]
    piece = lax.all_gather(arrived, "tp", axis=2, tiled=True)
    gate_val = jnp.einsum("erd,edf->erf", piece, gate_new, preferred_element_type=jnp.float32)
    up_val = jnp.einsum("erd,edf->erf", piece, up_new, preferred_element_type=jnp.float32)
    hidden = (jax.nn.silu(gate_val) * up_val).astype(jnp.bfloat16)
    own_width = model_width // tp_count
    summed_rows = jnp.einsum(
        "erf,efc->erc",
        lax.all_gather(hidden, "tp", axis=2, tiled=True),
        down_cols,
        preferred_element_type=jnp.float32,
    )
    summed = jnp.transpose(summed_rows, (2, 0, 1)).reshape(own_width, -1)
    outgoing_back = summed.astype(jnp.bfloat16).reshape(
        own_width, local_experts, fs_count, capacity
    )
    returned = lax.all_to_all(outgoing_back, "fs", split_axis=2, concat_axis=1, tiled=True)
    returned_rows = returned.reshape(own_width, experts_all * capacity)
    picked = jnp.take(returned_rows, targets, axis=1).astype(jnp.float32)
    weights = group_weight[:, None] * expert_share / jnp.sum(expert_share, axis=1, keepdims=True)
    mixed = jnp.sum(picked * weights[None, :, :], axis=2)
    return (mixed.T.astype(jnp.bfloat16), gate_new, up_new, down_new)


def solution(mesh):
    placed = (
        P("fs", None),
        P("fs", None),
        P("fs"),
        P("fs", None),
        P("fs"),
        P(None, "fs", "tp"),
        P(None, "fs", "tp"),
        P(None, "fs", "tp"),
    )
    return jax.shard_map(
        on_device,
        mesh=mesh,
        in_specs=placed,
        out_specs=(P("fs", "tp"), P("fs", None, "tp"), P("fs", None, "tp"), P("fs", "tp", None)),
        check_vma=False,
    )
```

profile of v0, /device:TPU:0, one launch (start us, length us, event | category | flops | bytes accessed | tf_op | source)
XLA Modules:
  0.0 568.2 jit_solution(14074407424109745335)
XLA Ops:
  8.4 6.7 %convert_element_type.52 = f32[512,4096]{1,0:T(8,128)} convert(bf16[512,4096]{1,0:T(8,128)(2,1)} %param.8) | non-fusion elementwise | flops 2097152 | bytes 12582912 | tf_op jit(solution)/shard_map/convert_element_type | solution.py:29
  16.0 4.5 reduce-window.6
  26.3 77.8 %all_to_all.102 = bf16[8,2,96,1024]{3,2,1,0:T(8,128)(2,1)S(1)} all-to-all(bf16[8,2,96,1024]{3,2,1,0:T(8,128)(2,1)S(1)} %bitcast.59), channel_id=1, replica_groups=mesh['fs'=8,'tp'=4] {'fs'}, dimensions={0} | all-to-all | bytes 6291456 | tf_op jit(solution)/shard_map/all_to_all | solution.py:46
  106.2 9.3 %multiply_convert_fusion = (bf16[16,512,256]{2,1,0:T(8,128)(2,1)}, bf16[16,512,256]{2,1,0:T(8,128)(2,1)S(1)}) fusion(f32[16,512,256]{2,1,0:T(8,128)} %param.14, f32[512]{0:T(512)S(1)} %copy-done.7, f32[16,512,256]{2,1,0:T(8,128)} %param.13), kind=kLoop, calls=%fused_computation.1 | loop fusion | flops 8388608 | bytes 25167872 | tf_op jit(solution)/shard_map/convert_element_type | solution.py:14
  115.5 96.2 %all_to_all.103 = bf16[16,512,256]{2,1,0:T(8,128)(2,1)} all-to-all(bf16[16,512,256]{2,1,0:T(8,128)(2,1)S(1)} %get-tuple-element.7), channel_id=1, replica_groups=mesh['fs'=8,'tp'=4] {'fs'}, dimensions={0} | all-to-all | bytes 8388608 | tf_op jit(solution)/shard_map/all_to_all | solution.py:16
  211.7 4.6 all-to-all-start.2
  216.3 6.0 %convert_element_type.58 = bf16[16,128,1024]{2,1,0:T(8,128)(2,1)} convert(f32[16,128,1024]{2,1,0:T(8,128)} %param.15) | non-fusion elementwise | flops 2097152 | bytes 12582912 | tf_op jit(solution)/shard_map/convert_element_type | solution.py:20
  222.2 86.2 %all-to-all-done.2 = bf16[16,512,256]{2,1,0:T(8,128)(2,1)} async-done(((bf16[16,512,256]{2,1,0:T(8,128)(2,1)}), bf16[16,512,256]{2,1,0:T(8,128)(2,1)}, u32[]{:S(2)}, u32[]{:S(2)}) %all-to-all-start.2) | async-done | bytes 4194336 | tf_op jit(solution)/shard_map/all_to_all | solution.py:17
  308.5 4.6 all-to-all-start.3
  313.3 4.6 copy.72
  317.9 4.6 copy.73
  322.5 7.8 %fusion.9 = f32[2,768,256]{2,1,0:T(8,128)S(1)} fusion(bf16[2,768,4096]{2,1,0:T(8,128)(2,1)} %all-gather.3.cloned.1.call-done, bf16[2,4096,256]{2,1,0:T(8,128)(2,1)} %bitcast.55), kind=kOutput, calls=%fused_computation.29 | convolution fusion | flops 3221225472 | bytes 18350080 | tf_op jit(solution)/shard_map/erd,edf->erf/dot_general | solution.py:54
  333.1 4.5 multiply_convert_fusion.2
  337.6 67.9 %all-to-all-done.3 = bf16[16,128,1024]{2,1,0:T(8,128)(2,1)} async-done(((bf16[16,128,1024]{2,1,0:T(8,128)(2,1)}), bf16[16,128,1024]{2,1,0:T(8,128)(2,1)}, u32[]{:S(2)}, u32[]{:S(2)}) %all-to-all-start.3) | async-done | bytes 4194336 | tf_op jit(solution)/shard_map/all_to_all | solution.py:19
  410.2 6.3 %copy.78 = bf16[2,1024,1024]{2,0,1:T(2,128)(2,1)} copy(bf16[2,1024,1024]{2,1,0:T(8,128)(2,1)S(1)} %bitcast.51) | data formatting | bytes 8388608 | tf_op jit(solution)/shard_map/all_to_all | solution.py:19
  416.5 5.1 all-to-all-start.5
  421.6 6.6 %convolution_convert_fusion.1 = bf16[2,768,1024]{2,1,0:T(8,128)(2,1)S(1)} fusion(bf16[2,768,1024]{2,1,0:T(8,128)(2,1)} %all-gather.5.cloned.1.call-done, bf16[2,1024,1024]{2,1,0:T(8,128)(2,1)} %bitcast.52), kind=kOutput, calls=%fused_computation.10 | convolution fusion | flops 3222798336 | bytes 10485760 | tf_op jit(solution)/shard_map/erf,efc->erc/dot_general | solution.py:58
  430.3 39.3 %all-to-all-done.5 = bf16[2,1024,1024]{2,0,1:T(2,128)(2,1)} async-done(((bf16[2,1024,1024]{2,0,1:T(2,128)(2,1)}), bf16[2,1024,1024]{2,0,1:T(2,128)(2,1)}, u32[]{:S(2)}, u32[]{:S(2)}) %all-to-all-start.5) | async-done | bytes 4194336 | tf_op jit(solution)/shard_map/all_to_all | solution.py:22
  469.6 3.6 all-to-all-start.4
  475.3 7.4 %copy.79 = bf16[2,256,4,1024]{3,2,1,0:T(4,128)(2,1)} copy(bf16[2,256,4,1024]{3,0,1,2:T(2,128)(2,1)} %bitcast.22) | data formatting | bytes 8388608 | tf_op jit(solution)/shard_map/all_to_all | solution.py:22
  482.7 7.8 %all_to_all.95 = bf16[2,256,4096]{2,1,0:T(8,128)(2,1)} reshape(bf16[2,256,4,1024]{3,2,1,0:T(4,128)(2,1)} %copy.79) | data formatting | bytes 8388608 | tf_op jit(solution)/shard_map/all_to_all | solution.py:22
  490.4 53.4 %all-to-all-done.4 = bf16[1024,2,8,96]{0,3,1,2:T(8,128)(2,1)S(1)} async-done(((bf16[1024,2,8,96]{0,3,1,2:T(8,128)(2,1)}), bf16[1024,2,8,96]{0,3,1,2:T(8,128)(2,1)S(1)}, u32[]{:S(2)}, u32[]{:S(2)}) %all-to-all-start.4) | async-done | bytes 3145760 | tf_op jit(solution)/shard_map/all_to_all | solution.py:68
  543.8 5.3 gather_fusion
  552.0 9.4 %multiply_reduce_fusion.1 = bf16[512,1024]{1,0:T(8,128)(2,1)} fusion(bf16[512,2,1024]{2,1,0:T(2,128)(2,1)S(1)} %reshape.73, pred[512,2]{1,0:T(8,128)(4,1)S(1)} %copy-done.4, f32[512,2]{1,0:T(8,128)S(1)} %copy-done.3), kind=kLoop, calls=%fused_computation.6 | loop fusion | flops 3670016 | bytes 3150848 | tf_op jit(solution)/shard_map/reduce_sum | solution.py:72
  (56 shorter events, 24.6 us)
Async XLA Ops:
  7.2 315.3 %all-gather.3.cloned.1.call-start = ((), (), s32[]{:S(2)}) async-start(), calls=%async_computation.6 | async-start | bytes 15728640 | tf_op jit(solution)/shard_map/all_gather | solution.py:53
  8.4 6.7 %copy-start = (bf16[512,4096]{1,0:T(8,128)(2,1)S(1)}, bf16[512,4096]{1,0:T(8,128)(2,1)}, u32[]{:S(2)}) copy-start(bf16[512,4096]{1,0:T(8,128)(2,1)} %param.8) | copy-start | bytes 12582916
  15.1 6.2 %copy-start.5 = (s32[512,2]{0,1:T(2,128)S(1)}, s32[512,2]{0,1:T(2,128)}, u32[]{:S(2)}) copy-start(s32[512,2]{0,1:T(2,128)} %param.9) | copy-start | bytes 12292
  104.1 2.1 copy-start.7
  211.7 96.8 %all-to-all-start.2 = ((bf16[16,512,256]{2,1,0:T(8,128)(2,1)}), bf16[16,512,256]{2,1,0:T(8,128)(2,1)}, u32[]{:S(2)}, u32[]{:S(2)}) async-start(bf16[16,512,256]{2,1,0:T(8,128)(2,1)} %get-tuple-element.6), calls=%async_computation.2 | async-start | bytes 8388608 | tf_op jit(solution)/shard_map/all_to_all | solution.py:17
  308.5 97.1 %all-to-all-start.3 = ((bf16[16,128,1024]{2,1,0:T(8,128)(2,1)}), bf16[16,128,1024]{2,1,0:T(8,128)(2,1)}, u32[]{:S(2)}, u32[]{:S(2)}) async-start(bf16[16,128,1024]{2,1,0:T(8,128)(2,1)} %convert_element_type.58), calls=%async_computation.3 | async-start | bytes 8388608 | tf_op jit(solution)/shard_map/all_to_all | solution.py:19
  313.1 108.5 %all-gather.5.cloned.1.call-start = ((), (), s32[]{:S(2)}) async-start(), calls=%async_computation.7 | async-start | bytes 3932160 | tf_op jit(solution)/shard_map/all_gather | solution.py:60
  322.5 7.8 %copy-start.2 = (bf16[8,2,512,256]{3,2,0,1:T(8,128)(2,1)S(1)}, bf16[8,2,512,256]{3,2,0,1:T(8,128)(2,1)}, u32[]{:S(2)}) copy-start(bf16[8,2,512,256]{3,2,0,1:T(8,128)(2,1)} %copy.73) | copy-start | bytes 12582916
  322.5 10.7 %copy-start.9 = (bf16[2,768,4096]{2,1,0:T(8,128)(2,1)S(1)}, bf16[2,768,4096]{2,1,0:T(8,128)(2,1)}, u32[]{:S(2)}) copy-start(bf16[2,768,4096]{2,1,0:T(8,128)(2,1)} %all-gather.3.cloned.1.call-done) | copy-start | bytes 37748740
  408.2 2.0 copy-start.1
  416.5 53.0 %all-to-all-start.5 = ((bf16[2,1024,1024]{2,0,1:T(2,128)(2,1)}), bf16[2,1024,1024]{2,0,1:T(2,128)(2,1)}, u32[]{:S(2)}, u32[]{:S(2)}) async-start(bf16[2,1024,1024]{2,0,1:T(2,128)(2,1)} %copy.78), calls=%async_computation.5 | async-start | bytes 8388608 | tf_op jit(solution)/shard_map/all_to_all | solution.py:22
  430.3 44.1 %copy-start.6 = (f32[512,2]{0,1:T(2,128)S(1)}, f32[512,2]{0,1:T(2,128)}, u32[]{:S(2)}) copy-start(f32[512,2]{0,1:T(2,128)} %param.11) | copy-start | bytes 12292
  430.3 44.1 %copy-start.8 = (f32[512]{0:T(512)S(1)}, f32[512]{0:T(512)}, u32[]{:S(2)}) copy-start(f32[512]{0:T(512)} %param.10) | copy-start | bytes 6148
  469.6 74.3 %all-to-all-start.4 = ((bf16[1024,2,8,96]{0,3,1,2:T(8,128)(2,1)}), bf16[1024,2,8,96]{0,3,1,2:T(8,128)(2,1)S(1)}, u32[]{:S(2)}, u32[]{:S(2)}) async-start(bf16[1024,2,8,96]{0,3,1,2:T(8,128)(2,1)} %copy.75), calls=%async_computation.4 | async-start | bytes 6291456 | tf_op jit(solution)/shard_map/all_to_all | solution.py:68
  549.2 2.8 copy-start.3
  549.2 2.8 copy-start.4
Sparse Core Ops, SparseCore 0:
  106.3 81.0 all-gather.2
  337.8 30.0 all-gather.4
where the time goes:
time: 569 us; the launch traced here: 568 us
  waiting for transfers between devices  247 us (43%)
  blocking collectives  174 us (31%)
  local copies, waits for them, and re-layouts  54.1 us (10%)
  other arithmetic  38.5 us (7%)
  matrix products  22.3 us (4%)
  starting transfers between devices  18.1 us (3%)
  between operations  14.3 us (3%)
    all_to_all x1, blocking collectives, on_device(): lax.all_to_all(gate_cast, 'fs', split_axis=0, concat_axis=1, tiled=True)  96.2 us
    all_to_all x1, waiting for transfers between devices, on_device(): lax.all_to_all(up_cast, 'fs', split_axis=0, concat_axis=1, tiled=True)  86.2 us
    all_to_all x1, blocking collectives, on_device(): lax.all_to_all(outgoing.reshape(fs_count, local_experts, capacity, own_co...  77.8 us
    all_to_all x1, waiting for transfers between devices, on_device(): lax.all_to_all(down_train.astype(jnp.bfloat16), 'fs', split_axis=0, conca...  67.9 us
    all_to_all x1, waiting for transfers between devices, on_device(): lax.all_to_all(outgoing_back, 'fs', split_axis=2, concat_axis=1, tiled=True)  53.4 us
    all_to_all x1, waiting for transfers between devices, on_device(): lax.all_to_all(down_cols, 'tp', split_axis=1, concat_axis=2, tiled=True)  39.3 us
    all_to_all x2, local copies, waits for them, and re-layouts, on_device(): lax.all_to_all(down_cols, 'tp', split_axis=1, concat_axis=2, tiled=True)  15.2 us
  transfers between devices with their start and end apart: 6, of which 4 were waited for; matrix products, arithmetic and copies ran while one was open for 11% of the time, Pallas kernels for 0%

commit v1 on v0

v1 whole, which is shorter than its diff:
```python
import jax
import jax.numpy as jnp
from jax import lax
from jax.experimental import pallas as pl
from jax.experimental.pallas import tpu as pltpu
from jax.sharding import PartitionSpec as P


EPS = 1e-06
BF = jnp.bfloat16
F32 = jnp.float32


def mark():
    def body(in_ref, out_ref):
        out_ref[...] = in_ref[...]

    pl.pallas_call(
        body,
        out_shape=jax.ShapeDtypeStruct((8, 128), F32),
        compiler_params=pltpu.CompilerParams(has_side_effects=True),
    )(jnp.zeros((8, 128), F32))


def swap(value, axis, bits):
    size = lax.axis_size(axis)
    return lax.ppermute(value, axis, [(i, i ^ bits) for i in range(size)])


def cut(value, start, size, axis):
    return lax.dynamic_slice_in_dim(value, start, size, axis, allow_negative_indices=False)


def tied(values, anchor):
    return lax.optimization_barrier((values, anchor))[0]


def spread(value):
    pieces = {0: value}
    bit = lax.axis_size("tp") // 2
    while bit:
        for distance, piece in list(pieces.items()):
            pieces[distance ^ bit] = swap(piece, "tp", bit)
        bit //= 2
    return pieces


def whole_vmem(count):
    return [pl.BlockSpec(memory_space=pltpu.VMEM)] * count


def combine(weights, blocks, total, dtype):
    tokens, slots = weights.shape
    cap, width = blocks[0].shape
    count = len(blocks)
    tile = min(256, width)

    def body(weights_ref, *refs):
        block_refs, refs = refs[:count], refs[count:]
        total_ref = None if total is None else refs[0]
        out_ref, whole = refs[-2], refs[-1]
        for q in range(count):
            whole[q * cap : (q + 1) * cap, :] = block_refs[q][...]

        @pl.loop(0, width // tile)
        def _(i):
            columns = pl.ds(pl.multiple_of(i * tile, tile), tile)
            term = jnp.dot(weights_ref[...], whole[:, columns], preferred_element_type=F32)
            if total_ref is not None:
                term = term + total_ref[:, columns]
            out_ref[:, columns] = term.astype(dtype)

    operands = [weights, *blocks] + ([] if total is None else [total])
    return pl.pallas_call(
        body,
        out_shape=jax.ShapeDtypeStruct((tokens, width), dtype),
        in_specs=whole_vmem(len(operands)),
        out_specs=whole_vmem(1)[0],
        scratch_shapes=[pltpu.VMEM((slots, width), BF)],
        cost_estimate=pl.CostEstimate(
            flops=2 * tokens * slots * width, bytes_accessed=2 * slots * width, transcendentals=0
        ),
    )(*operands)


def project(places, blocks, rows, gate=None):
    local, depth, cols = blocks[0].shape
    count = len(blocks)
    groups, parts = len(rows), len(rows[0])
    height, piece = rows[0][0].shape[1:]
    order = [m for m in sorted(rows[0])]
    flat = [group[m] for group in rows for m in order]

    def body(places_ref, *refs):
        block_refs, refs = refs[:count], refs[count:]
        row_refs, refs = refs[: len(flat)], refs[len(flat) :]
        gate_ref = None if gate is None else refs[0]
        whole_ref, out_ref = refs[-2:]
        me, tp = places_ref[0], places_ref[1]
        for k in range(count):
            spot = pl.ds(pl.multiple_of((me ^ k) * depth, depth), depth)
            whole_ref[0, spot, :] = block_refs[k][0]
        for g in range(groups):
            total = None
            for i, m in enumerate(order):
                spot = pl.ds(pl.multiple_of((tp ^ m) * piece, piece), piece)
                term = jnp.dot(
                    row_refs[g * parts + i][0],
                    whole_ref[0, spot, :],
                    preferred_element_type=F32,
                )
                total = term if total is None else total + term
            spot = slice(g * height, (g + 1) * height)
            if gate_ref is not None:
                value = gate_ref[0, spot, :]
                total = (value / (1.0 + jnp.exp(-value))) * total
            out_ref[0, spot, :] = total.astype(out_ref.dtype)

    def spec(*shape):
        return pl.BlockSpec((1,) + shape, lambda e, places: (e, 0, 0))

    many = groups * height
    return pl.pallas_call(
        body,
        grid_spec=pltpu.PrefetchScalarGridSpec(
            num_scalar_prefetch=1,
            grid=(local,),
            in_specs=[spec(depth, cols)] * count
            + [spec(height, piece)] * len(flat)
            + ([] if gate is None else [spec(many, cols)]),
            out_specs=[spec(depth * count, cols), spec(many, cols)],
        ),
        out_shape=[
            jax.ShapeDtypeStruct((local, depth * count, cols), BF),
            jax.ShapeDtypeStruct((local, many, cols), F32 if gate is None else BF),
        ],
        compiler_params=pltpu.CompilerParams(vmem_limit_bytes=48 << 20),
        cost_estimate=pl.CostEstimate(
            flops=2 * local * many * cols * piece * parts,
            bytes_accessed=4 * local * (depth * count * cols + many * piece),
            transcendentals=0,
        ),
    )(places, *blocks, *flat, *([] if gate is None else [gate]))


def lower(places, blocks, hidden, l, cap):
    depth, cols = blocks[0].shape
    count = len(blocks)
    order = [m for m in sorted(hidden)]
    parts = len(order)
    many, part = hidden[0].shape[1:]
    tile = min(256, cols)

    def body(places_ref, *refs):
        block_refs, refs = refs[:count], refs[count:]
        hidden_refs, refs = refs[:parts], refs[parts:]
        out_refs, refs = refs[:count], refs[count:]
        part_refs, whole = refs[:parts], refs[-1]
        me, tp = places_ref[0], places_ref[1]
        for k in range(count):
            spot = pl.ds(pl.multiple_of((me ^ k) * depth, depth), depth)
            whole[spot, :] = block_refs[k][...]

        @pl.loop(0, cols // tile)
        def _(i):
            columns = pl.ds(pl.multiple_of(i * tile, tile), tile)
            total = None
            for j, m in enumerate(order):
                spot = pl.ds(pl.multiple_of((tp ^ m) * part, part), part)
                weight = whole[spot, columns]
                part_refs[j][:, columns] = weight
                term = jnp.dot(hidden_refs[j][...], weight, preferred_element_type=F32)
                total = term if total is None else total + term
            total = total.astype(BF)
            for q in range(count):
                out_refs[q][:, columns] = total[q * cap : (q + 1) * cap]

    vmem = whole_vmem(1)[0]
    results = pl.pallas_call(
        body,
        in_specs=[pl.BlockSpec(memory_space=pltpu.SMEM)] + whole_vmem(count + parts),
        out_specs=[vmem] * (count + parts),
        out_shape=[jax.ShapeDtypeStruct((cap, cols), BF)] * count
        + [jax.ShapeDtypeStruct((part, cols), BF)] * parts,
        scratch_shapes=[pltpu.VMEM((depth * count, cols), BF)],
        compiler_params=pltpu.CompilerParams(vmem_limit_bytes=48 << 20),
        cost_estimate=pl.CostEstimate(
            flops=2 * many * cols * depth * count,
            bytes_accessed=4 * depth * count * cols,
            transcendentals=0,
        ),
    )(places, *blocks, *[hidden[m][l] for m in order])
    return results[:count], dict(zip(order, results[count:]))


def on_device(
    prompt, expert_ids, group_weight, expert_share, norm_gain, gate_train, up_train, down_train
):
    n = lax.axis_size("fs")
    parts = lax.axis_size("tp")
    me = lax.axis_index("fs")
    tp = lax.axis_index("tp")
    tokens, width = prompt.shape
    experts = gate_train.shape[0]
    local = experts // n
    cap = max(2, 3 * tokens // experts)
    half = n // 2
    piece = width // parts
    hidden_part = gate_train.shape[2]
    gain = norm_gain[None, :, None]

    def block(weights, k, scale=None):
        picked = cut(weights, (me ^ k) * local, local, 0)
        if scale is not None:
            picked = picked * scale
        return picked.astype(BF)

    near = list(range(1, half))
    far = list(range(half, n))

    ids = expert_ids.T
    expert_row = lax.broadcasted_iota(jnp.int32, (experts, tokens), 0)
    named = [ids[k][None, :] == expert_row for k in range(2)]
    chosen = named[0] | named[1]
    before = (
        lax.broadcasted_iota(jnp.int32, (tokens, tokens), 0)
        < lax.broadcasted_iota(jnp.int32, (tokens, tokens), 1)
    ).astype(BF)
    count = jnp.dot(chosen.astype(BF), before, preferred_element_type=F32)
    rank = jnp.where(chosen, count, -1.0).astype(BF)
    rank_other = swap(rank, "fs", half)

    wide = prompt.astype(F32)
    scale = lax.rsqrt(jnp.mean(wide * wide, axis=-1, keepdims=True) + EPS)
    own = cut(prompt, tp * piece, piece, 1)
    own = (own.astype(F32) * scale).astype(BF)
    other = swap(own, "fs", half)

    slot_row = lax.broadcasted_iota(jnp.int32, (1, cap, 1), 1).astype(BF)

    def pick(ranks, values, j):
        rows = cut(ranks, (me ^ j) * local, local, 0)
        mask = (rows[:, None, :] == slot_row).astype(BF).reshape(local * cap, tokens)
        got = jnp.dot(mask, values, preferred_element_type=F32).astype(BF)
        return got.reshape(local, cap, piece)

    places = jnp.stack([me, tp]).astype(jnp.int32)

    def route(ranks, values):
        got = [pick(ranks, values, j) for j in range(half)]
        rows = [swap(got[j], "fs", j) if j else got[0] for j in range(half)]
        return jnp.concatenate(rows, axis=1), got[half - 1]

    rows_a, _ = route(rank, own)
    gate_got = {k: block(gate_train, k, gain) for k in range(n)}
    for k in near:
        gate_got[k] = swap(gate_got[k], "fs", k)
    for k in far[:1]:
        gate_got[k] = swap(gate_got[k], "fs", k)
    mark()

    rows_b, anchor = route(rank_other, other)
    for k in far[1:]:
        gate_got[k] = swap(tied(gate_got[k], anchor), "fs", k)
    rows = [spread(rows_a)]
    mark()

    rows.append(spread(rows_b))
    up_got = {k: tied(block(up_train, k, gain), rows_b) for k in range(n)}
    for k in far + near:
        up_got[k] = swap(up_got[k], "fs", k)
    mark()

    def bring(l, anchor):
        got = {}
        for k in [0] + far + near:
            part = tied(cut(down_train, (me ^ k) * local + l, 1, 0)[0].astype(BF), anchor)
            got[k] = swap(part, "fs", k) if k else part
        return [got[k] for k in range(n)]

    down_got = [bring(l, rows[1][parts // 2]) for l in range(local - 1)]
    mark()

    gate_new, gate_val = project(places, [gate_got[k] for k in range(n)], rows)
    up_new, hidden = project(places, [up_got[k] for k in range(n)], rows, gate_val)
    down_got.append(bring(local - 1, gate_val))
    hidden_by = spread(hidden)
    mark()

    share = group_weight[:, None] * expert_share / jnp.sum(expert_share, axis=1, keepdims=True)
    share = share.T
    weight = jnp.where(named[0], share[0][None, :], 0.0) + jnp.where(
        named[1], share[1][None, :], 0.0
    )
    column = lax.broadcasted_iota(jnp.int32, (experts, n * cap), 1)
    row = lax.broadcasted_iota(jnp.int32, (experts, n * cap), 0)
    slot_col = (lax.broadcasted_iota(jnp.int32, (tokens, n * cap), 1) % cap).astype(F32)

    def combiner(l):
        expand = (row == (me ^ (column // cap)) * local + l).astype(BF)
        contract = (((0,), (0,)), ((), ()))
        ranks = lax.dot_general(rank, expand, contract, preferred_element_type=F32)
        weights = lax.dot_general(
            weight.astype(BF), expand, contract, preferred_element_type=F32
        )
        return jnp.where(ranks == slot_col, weights, 0.0).astype(BF)

    total = None
    down_new = jnp.zeros((local, hidden_part, width), BF)
    for l in range(local):
        last = l == local - 1
        out, sent = lower(places, down_got[l], hidden_by, l, cap)
        back = {}
        for q in [0] + far + near:
            back[q] = swap(out[q], "fs", q) if q else out[q]
        for m in range(1, parts):
            sent[m] = swap(sent[m], "tp", m)
        mark()
        for m in range(parts):
            down_new = lax.dynamic_update_slice(
                down_new,
                sent[m][None],
                (l, 0, (tp ^ m) * piece),
                allow_negative_indices=False,
            )
        total = combine(
            combiner(l), [back[q] for q in range(n)], total, BF if last else F32
        )
    return (total, gate_new, up_new, down_new)


def solution(mesh):
    placed = (
        P("fs", None),
        P("fs", None),
        P("fs"),
        P("fs", None),
        P("fs"),
        P(None, "fs", "tp"),
        P(None, "fs", "tp"),
        P(None, "fs", "tp"),
    )
    return jax.shard_map(
        on_device,
        mesh=mesh,
        in_specs=placed,
        out_specs=(P("fs", "tp"), P("fs", None, "tp"), P("fs", None, "tp"), P("fs", "tp", None)),
        check_vma=False,
    )
```

time: 569 us -> 536 us (0.942)
  blocking collectives: 174 us -> 0 us
  starting transfers between devices: 18.1 us -> 145 us
  waiting for transfers between devices: 247 us -> 299 us
  Pallas kernels: 0 us -> 44.2 us
  local copies, waits for them, and re-layouts: 54.1 us -> 23.2 us
  other arithmetic: 38.5 us -> 15.9 us
  matrix products: 22.3 us -> 6.88 us
  between operations: 14.3 us -> 1.05 us
    ppermute x0 -> x65, waiting for transfers between devices: none -> 299 us  [swap(): return lax.ppermute(value, axis, [(i, i ^ bits) for i in range(size)])]
    all_to_all x4 -> x0, waiting for transfers between devices: 247 us -> none  [the longest x1 86.2 us: on_device(): lax.all_to_all(up_cast, 'fs', split_axis=0, concat_axis=1, tiled=True)]
    all_to_all x2 -> x0, blocking collectives: 174 us -> none  [the longest x1 96.2 us: on_device(): lax.all_to_all(gate_cast, 'fs', split_axis=0, concat_axis=1, tiled=True)]
    ppermute x0 -> x65, starting transfers between devices: none -> 145 us  [swap(): return lax.ppermute(value, axis, [(i, i ^ bits) for i in range(size)])]
    pallas_call x0 -> x13, Pallas kernels: none -> 44.2 us  [the longest x2 17.1 us: project(): pl.pallas_call(body, grid_spec=pltpu.PrefetchScalarGridSpec(num_scalar_pr...]
    all_to_all x7 -> x0, local copies, waits for them, and re-layouts: 35.3 us -> none  [the longest x2 15.2 us: on_device(): lax.all_to_all(down_cols, 'tp', split_axis=1, concat_axis=2, tiled=True)]
    all_to_all x4 -> x0, starting transfers between devices: 17.8 us -> none  [the longest x1 5.06 us: on_device(): lax.all_to_all(down_cols, 'tp', split_axis=1, concat_axis=2, tiled=True)]
    dot_general x4 -> x13, matrix products: 22.3 us -> 6.88 us  [the longest x8 3.35 us: pick(): got = jnp.dot(mask, values, preferred_element_type=F32).astype(BF)]
  transfers between devices with their start and end apart: 6 -> 65, of which waited for: 4 -> 25; matrix products, arithmetic and copies ran while one was open for 11% -> 6% of each run, Pallas kernels for 0% -> 7%
where the time goes in v1:
time: 536 us; the launch traced here: 535 us
  waiting for transfers between devices  299 us (56%)
  starting transfers between devices  145 us (27%)
  Pallas kernels  44.2 us (8%)
  local copies, waits for them, and re-layouts  23.2 us (4%)
  other arithmetic  15.9 us (3%)
  matrix products  6.88 us (1%)
    ppermute x65, waiting for transfers between devices, swap(): return lax.ppermute(value, axis, [(i, i ^ bits) for i in range(size)])  299 us
    ppermute x65, starting transfers between devices, swap(): return lax.ppermute(value, axis, [(i, i ^ bits) for i in range(size)])  145 us
    pallas_call x2, Pallas kernels, project(): pl.pallas_call(body, grid_spec=pltpu.PrefetchScalarGridSpec(num_scalar_pr...  17.1 us
    unnamed x48, local copies, waits for them, and re-layouts  10.9 us
  transfers between devices with their start and end apart: 65, of which 25 were waited for; matrix products, arithmetic and copies ran while one was open for 6% of the time, Pallas kernels for 7%

profile of v1, /device:TPU:0, one launch (start us, length us, event | category | flops | bytes accessed | tf_op | source)
XLA Modules:
  0.0 534.9 jit_solution(16834529689928934871)
XLA Ops:
  16.0 42.4 %collective-permute-done.5 = bf16[512,1024]{1,0:T(8,128)(2,1)S(1)} collective-permute-done((bf16[512,1024]{1,0:T(8,128)(2,1)S(1)}, bf16[512,1024]{1,0:T(8,128)(2,1)S(1)}, u32[]{:S(2)}, u32[]{:S(2)}) %collective-permute-start.5) | collective-permute-done | bytes 1048608 | tf_op jit(solution)/shard_map/ppermute | solution.py:27
  81.1 8.7 %multiply_convert_fusion.1 = (bf16[2,512,256]{2,1,0:T(8,128)(2,1)}, bf16[2,512,256]{2,1,0:T(8,128)(2,1)}, bf16[2,512,256]{2,1,0:T(8,128)(2,1)}, bf16[2,512,256]{...) fusion(f32[16,512,256]{2,1,0:T(8,128)} %param.14, ...), kind=kLoop, calls=%fused_computation.18 | loop fusion | flops 8388608 | bytes 25167904 | tf_op jit(solution)/shard_map/convert_element_type | solution.py:216
  93.4 10.4 %collective-permute-done.refs_1_ = bf16[2,512,256]{2,1,0:T(8,128)(2,1)S(1)} collective-permute-done((bf16[2,512,256]{2,1,0:T(8,128)(2,1)S(1)}, bf16[2,512,256]{2,1,0:T(8,128)(2,1)S(1)}, u32[]{:S(2)}, u32[]{:S(2)}) %collective-permute-start) | collective-permute-done | bytes 524320 | tf_op jit(solution)/shard_map/ppermute | solution.py:27
  104.7 11.8 %collective-permute-done.1.refs_2_ = bf16[2,512,256]{2,1,0:T(8,128)(2,1)S(1)} collective-permute-done((bf16[2,512,256]{2,1,0:T(8,128)(2,1)S(1)}, bf16[2,512,256]{2,1,0:T(8,128)(2,1)S(1)}, u32[]{:S(2)}, u32[]{:S(2)}) %collective-permute-start.1) | collective-permute-done | bytes 524320 | tf_op jit(solution)/shard_map/ppermute | solution.py:27
  116.5 9.1 %collective-permute-done.2.refs_3_ = bf16[2,512,256]{2,1,0:T(8,128)(2,1)S(1)} collective-permute-done((bf16[2,512,256]{2,1,0:T(8,128)(2,1)S(1)}, bf16[2,512,256]{2,1,0:T(8,128)(2,1)S(1)}, u32[]{:S(2)}, u32[]{:S(2)}) %collective-permute-start.2) | collective-permute-done | bytes 524320 | tf_op jit(solution)/shard_map/ppermute | solution.py:27
  127.3 31.5 %collective-permute-done.3.refs_4_ = bf16[2,512,256]{2,1,0:T(8,128)(2,1)S(1)} collective-permute-done((bf16[2,512,256]{2,1,0:T(8,128)(2,1)S(1)}, bf16[2,512,256]{2,1,0:T(8,128)(2,1)S(1)}, u32[]{:S(2)}, u32[]{:S(2)}) %collective-permute-start.3) | collective-permute-done | bytes 524320 | tf_op jit(solution)/shard_map/ppermute | solution.py:27
  161.5 14.7 %collective-permute-done.6.refs_5_ = bf16[2,512,256]{2,1,0:T(8,128)(2,1)S(1)} collective-permute-done((bf16[2,512,256]{2,1,0:T(8,128)(2,1)S(1)}, bf16[2,512,256]{2,1,0:T(8,128)(2,1)S(1)}, u32[]{:S(2)}, u32[]{:S(2)}) %collective-permute-start.6) | collective-permute-done | bytes 524320 | tf_op jit(solution)/shard_map/ppermute | solution.py:27
  180.6 12.9 %collective-permute-done.28.refs_1_ = bf16[2,512,256]{2,1,0:T(8,128)(2,1)S(1)} collective-permute-done((bf16[2,512,256]{2,1,0:T(8,128)(2,1)S(1)}, bf16[2,512,256]{2,1,0:T(8,128)(2,1)S(1)}, u32[]{:S(2)}, u32[]{:S(2)}) %collective-permute-start.28) | collective-permute-done | bytes 524320 | tf_op jit(solution)/shard_map/ppermute | solution.py:27
  194.3 14.8 %collective-permute-start.29 = (bf16[2,512,256]{2,1,0:T(8,128)(2,1)}, bf16[2,512,256]{2,1,0:T(8,128)(2,1)}, u32[]{:S(2)}, u32[]{:S(2)}) collective-permute-start(bf16[2,512,256]{2,1,0:T(8,128)(2,1)} %get-tuple-element.73), channel_id=1, source_target_pairs={{0,8},{4,12},{8,0},{12,4},{16,24},{20,28},{24,16},{28,20},{1,9},{5... | collective-permute-start | bytes 1572872 | tf_op jit(solution)/shard_map/ppermute | solution.py:27
  209.2 9.8 %collective-permute-done.29.refs_2_ = bf16[2,512,256]{2,1,0:T(8,128)(2,1)} collective-permute-done((bf16[2,512,256]{2,1,0:T(8,128)(2,1)}, bf16[2,512,256]{2,1,0:T(8,128)(2,1)}, u32[]{:S(2)}, u32[]{:S(2)}) %collective-permute-start.29) | collective-permute-done | bytes 524320 | tf_op jit(solution)/shard_map/ppermute | solution.py:27
  231.0 8.4 %shard_map.118 = (bf16[2,4096,256]{2,1,0:T(8,128)(2,1)}, f32[2,768,256]{2,1,0:T(8,128)S(1)}) custom-call(s32[2]{0:T(128)S(1)} %pad_add_fusion.places_ref, bf16[2,512,256]{2,1,0:T(8,128)(2,1)S(1)} %get-tuple-element.167.refs_0_, bf16[2,512,256]{2,1,0:T(8,128)(2,1)S(1)} %collective-permute-done.refs_1_, ...), custom_call_target="tpu_custom_call" | custom-call | flops 3221225472 | bytes 14680064 | tf_op jit(solution)/shard_map/pallas_call | solution.py:123
  240.6 40.5 %collective-permute-done.31.refs_4_ = bf16[2,512,256]{2,1,0:T(8,128)(2,1)S(1)} collective-permute-done((bf16[2,512,256]{2,1,0:T(8,128)(2,1)}, bf16[2,512,256]{2,1,0:T(8,128)(2,1)S(1)}, u32[]{:S(2)}, u32[]{:S(2)}) %collective-permute-start.31) | collective-permute-done | bytes 524320 | tf_op jit(solution)/shard_map/ppermute | solution.py:27
  281.1 12.1 %collective-permute-done.32.refs_5_ = bf16[2,512,256]{2,1,0:T(8,128)(2,1)S(1)} collective-permute-done((bf16[2,512,256]{2,1,0:T(8,128)(2,1)}, bf16[2,512,256]{2,1,0:T(8,128)(2,1)S(1)}, u32[]{:S(2)}, u32[]{:S(2)}) %collective-permute-start.32) | collective-permute-done | bytes 524320 | tf_op jit(solution)/shard_map/ppermute | solution.py:27
  293.2 8.7 %shard_map.119 = (bf16[2,4096,256]{2,1,0:T(8,128)(2,1)}, bf16[2,768,256]{2,1,0:T(8,128)(2,1)S(1)}) custom-call(s32[2]{0:T(128)S(1)} %pad_add_fusion.places_ref, bf16[2,512,256]{2,1,0:T(8,128)(2,1)S(1)} %get-tuple-element.71.refs_0_, bf16[2,512,256]{2,1,0:T(8,128)(2,1)S(1)} %copy-done.8, bf16[2,512,256]{2,1,0:T(8,128)(2,1)} %collective-permute-done.29.refs_2_, ...), custom_call_target="tpu_custom_call" | custom-call | flops 3221225472 | bytes 14680064 | tf_op jit(solution)/shard_map/pallas_call | solution.py:123
  307.7 17.1 %collective-permute-start.46 = (bf16[128,1024]{1,0:T(8,128)(2,1)S(1)}, bf16[128,1024]{1,0:T(8,128)(2,1)S(1)}, u32[]{:S(2)}, u32[]{:S(2)}) collective-permute-start(bf16[128,1024]{1,0:T(8,128)(2,1)S(1)} %get-tuple-element.90), channel_id=1, source_target_pairs={{0,8},{4,12},{8,0},{12,4},{16,24},{20,28},{24,16},{28,20},{1,9},{5... | collective-permute-start | bytes 786440 | tf_op jit(solution)/shard_map/ppermute | solution.py:27
  325.6 7.8 %collective-permute-start.48 = (bf16[128,1024]{1,0:T(8,128)(2,1)S(1)}, bf16[128,1024]{1,0:T(8,128)(2,1)S(1)}, u32[]{:S(2)}, u32[]{:S(2)}) collective-permute-start(bf16[128,1024]{1,0:T(8,128)(2,1)S(1)} %get-tuple-element.92), channel_id=1, source_target_pairs={{0,16},{4,20},{8,24},{12,28},{16,0},{20,4},{24,8},{28,12},{1,17},{... | collective-permute-start | bytes 786440 | tf_op jit(solution)/shard_map/ppermute | solution.py:27
  346.5 16.6 %collective-permute-done.48.refs_4_ = bf16[128,1024]{1,0:T(8,128)(2,1)S(1)} collective-permute-done((bf16[128,1024]{1,0:T(8,128)(2,1)S(1)}, bf16[128,1024]{1,0:T(8,128)(2,1)S(1)}, u32[]{:S(2)}, u32[]{:S(2)}) %collective-permute-start.48) | collective-permute-done | bytes 262176 | tf_op jit(solution)/shard_map/ppermute | solution.py:27
  364.9 9.7 %collective-permute-done.49.refs_5_ = bf16[128,1024]{1,0:T(8,128)(2,1)S(1)} collective-permute-done((bf16[128,1024]{1,0:T(8,128)(2,1)S(1)}, bf16[128,1024]{1,0:T(8,128)(2,1)S(1)}, u32[]{:S(2)}, u32[]{:S(2)}) %collective-permute-start.49) | collective-permute-done | bytes 262176 | tf_op jit(solution)/shard_map/ppermute | solution.py:27
  376.2 10.3 %collective-permute-start.25 = (bf16[128,1024]{1,0:T(8,128)(2,1)S(1)}, bf16[128,1024]{1,0:T(8,128)(2,1)S(1)}, u32[]{:S(2)}, u32[]{:S(2)}) collective-permute-start(bf16[128,1024]{1,0:T(8,128)(2,1)S(1)} %get-tuple-element.68), channel_id=1, source_target_pairs={{0,20},{4,16},{8,28},{12,24},{16,4},{20,0},{24,12},{28,8},{1,21},{... | collective-permute-start | bytes 786440 | tf_op jit(solution)/shard_map/ppermute | solution.py:27
  386.6 17.3 %collective-permute-start.23 = (bf16[128,1024]{1,0:T(8,128)(2,1)S(1)}, bf16[128,1024]{1,0:T(8,128)(2,1)S(1)}, u32[]{:S(2)}, u32[]{:S(2)}) collective-permute-start(bf16[128,1024]{1,0:T(8,128)(2,1)S(1)} %get-tuple-element.66), channel_id=1, source_target_pairs={{0,12},{4,8},{8,4},{12,0},{16,28},{20,24},{24,20},{28,16},{1,13},{... | collective-permute-start | bytes 786440 | tf_op jit(solution)/shard_map/ppermute | solution.py:27
  412.1 8.6 %collective-permute-done.25.refs_5_ = bf16[128,1024]{1,0:T(8,128)(2,1)S(1)} collective-permute-done((bf16[128,1024]{1,0:T(8,128)(2,1)S(1)}, bf16[128,1024]{1,0:T(8,128)(2,1)S(1)}, u32[]{:S(2)}, u32[]{:S(2)}) %collective-permute-start.25) | collective-permute-done | bytes 262176 | tf_op jit(solution)/shard_map/ppermute | solution.py:27
  445.1 9.5 %collective-permute-done.55.refs_4_ = bf16[96,1024]{1,0:T(8,128)(2,1)S(1)} collective-permute-done((bf16[96,1024]{1,0:T(8,128)(2,1)S(1)}, bf16[96,1024]{1,0:T(8,128)(2,1)S(1)}, u32[]{:S(2)}, u32[]{:S(2)}) %collective-permute-start.55) | collective-permute-done | bytes 196640 | tf_op jit(solution)/shard_map/ppermute | solution.py:27
  514.1 9.3 %collective-permute-done.63 = bf16[256,1024]{1,0:T(8,128)(2,1)S(1)} collective-permute-done((bf16[256,1024]{1,0:T(8,128)(2,1)}, bf16[256,1024]{1,0:T(8,128)(2,1)S(1)}, u32[]{:S(2)}, u32[]{:S(2)}) %collective-permute-start.63) | collective-permute-done | bytes 524320 | tf_op jit(solution)/shard_map/ppermute | solution.py:27
  524.2 9.8 %collective-permute-done.64 = bf16[256,1024]{1,0:T(8,128)(2,1)S(1)} collective-permute-done((bf16[256,1024]{1,0:T(8,128)(2,1)}, bf16[256,1024]{1,0:T(8,128)(2,1)S(1)}, u32[]{:S(2)}, u32[]{:S(2)}) %collective-permute-start.64) | collective-permute-done | bytes 524320 | tf_op jit(solution)/shard_map/ppermute | solution.py:27
  (222 shorter events, 182.1 us)
Async XLA Ops:
  10.3 48.1 %collective-permute-start.5 = (bf16[512,1024]{1,0:T(8,128)(2,1)S(1)}, bf16[512,1024]{1,0:T(8,128)(2,1)S(1)}, u32[]{:S(2)}, u32[]{:S(2)}) collective-permute-start(bf16[512,1024]{1,0:T(8,128)(2,1)S(1)} %multiply_convert_fusion), channel_id=1, source_target_pairs={{0,16},{4,20},{8,24},{12,28},{16,0},{20,4},{24,8},{28,12},{1,17},{... | collective-permute-start | bytes 3145736 | tf_op jit(solution)/shard_map/ppermute | solution.py:27
  10.9 50.4 %collective-permute-start.10 = (bf16[2,96,1024]{2,1,0:T(8,128)(2,1)S(1)}, bf16[2,96,1024]{2,1,0:T(8,128)(2,1)S(1)}, u32[]{:S(2)}, u32[]{:S(2)}) collective-permute-start(bf16[2,96,1024]{2,1,0:T(8,128)(2,1)S(1)} %bitcast.109), channel_id=1, source_target_pairs={{0,8},{4,12},{8,0},{12,4},{16,24},{20,28},{24,16},{28,20},{1,9},{5... | collective-permute-start | bytes 1179656 | tf_op jit(solution)/shard_map/ppermute | solution.py:27
  13.3 50.1 %collective-permute-start.11 = (bf16[2,96,1024]{2,1,0:T(8,128)(2,1)S(1)}, bf16[2,96,1024]{2,1,0:T(8,128)(2,1)S(1)}, u32[]{:S(2)}, u32[]{:S(2)}) collective-permute-start(bf16[2,96,1024]{2,1,0:T(8,128)(2,1)S(1)} %bitcast.110), channel_id=1, source_target_pairs={{0,12},{4,8},{8,4},{12,0},{16,28},{20,24},{24,20},{28,16},{1,13},{... | collective-permute-start | bytes 1179656 | tf_op jit(solution)/shard_map/ppermute | solution.py:27
  15.2 48.2 %collective-permute-start.9 = (bf16[2,96,1024]{2,1,0:T(8,128)(2,1)S(1)}, bf16[2,96,1024]{2,1,0:T(8,128)(2,1)S(1)}, u32[]{:S(2)}, u32[]{:S(2)}) collective-permute-start(bf16[2,96,1024]{2,1,0:T(8,128)(2,1)S(1)} %bitcast.111), channel_id=1, source_target_pairs={{0,4},{4,0},{8,12},{12,8},{16,20},{20,16},{24,28},{28,24},{1,5},{5... | collective-permute-start | bytes 1179656 | tf_op jit(solution)/shard_map/ppermute | solution.py:27
  64.7 113.6 %collective-permute-start.13 = (bf16[2,384,1024]{2,1,0:T(8,128)(2,1)}, bf16[2,384,1024]{2,1,0:T(8,128)(2,1)}, u32[]{:S(2)}, u32[]{:S(2)}) collective-permute-start(bf16[2,384,1024]{2,1,0:T(8,128)(2,1)} %pad_maximum_fusion.refs_8_), channel_id=1, source_target_pairs={{0,2},{1,3},{2,0},{3,1},{4,6},{5,7},{6,4},{7,5},{8,10},{9,11},{10,... | collective-permute-start | bytes 4718600 | tf_op jit(solution)/shard_map/ppermute | solution.py:27
  79.6 98.7 %collective-permute-start.19 = (bf16[2,384,1024]{2,1,0:T(8,128)(2,1)}, bf16[2,384,1024]{2,1,0:T(8,128)(2,1)}, u32[]{:S(2)}, u32[]{:S(2)}) collective-permute-start(bf16[2,384,1024]{2,1,0:T(8,128)(2,1)} %pad_maximum_fusion.1.refs_12_), channel_id=1, source_target_pairs={{0,2},{1,3},{2,0},{3,1},{4,6},{5,7},{6,4},{7,5},{8,10},{9,11},{10,... | collective-permute-start | bytes 4718600 | tf_op jit(solution)/shard_map/ppermute | solution.py:27
  103.8 55.0 %collective-permute-start.3 = (bf16[2,512,256]{2,1,0:T(8,128)(2,1)S(1)}, bf16[2,512,256]{2,1,0:T(8,128)(2,1)S(1)}, u32[]{:S(2)}, u32[]{:S(2)}) collective-permute-start(bf16[2,512,256]{2,1,0:T(8,128)(2,1)S(1)} %get-tuple-element.171), channel_id=1, source_target_pairs={{0,16},{4,20},{8,24},{12,28},{16,0},{20,4},{24,8},{28,12},{1,17},{... | collective-permute-start | bytes 1572872 | tf_op jit(solution)/shard_map/ppermute | solution.py:27
  116.5 59.6 %collective-permute-start.6 = (bf16[2,512,256]{2,1,0:T(8,128)(2,1)S(1)}, bf16[2,512,256]{2,1,0:T(8,128)(2,1)S(1)}, u32[]{:S(2)}, u32[]{:S(2)}) collective-permute-start(bf16[2,512,256]{2,1,0:T(8,128)(2,1)S(1)} %get-tuple-element.59), channel_id=1, source_target_pairs={{0,20},{4,16},{8,28},{12,24},{16,4},{20,0},{24,12},{28,8},{1,21},{... | collective-permute-start | bytes 1572872 | tf_op jit(solution)/shard_map/ppermute | solution.py:27
  125.7 51.3 %collective-permute-start.7 = (bf16[2,512,256]{2,1,0:T(8,128)(2,1)S(1)}, bf16[2,512,256]{2,1,0:T(8,128)(2,1)S(1)}, u32[]{:S(2)}, u32[]{:S(2)}) collective-permute-start(bf16[2,512,256]{2,1,0:T(8,128)(2,1)S(1)} %get-tuple-element.60), channel_id=1, source_target_pairs={{0,24},{4,28},{8,16},{12,20},{16,8},{20,12},{24,0},{28,4},{1,25},{... | collective-permute-start | bytes 1572872 | tf_op jit(solution)/shard_map/ppermute | solution.py:27
  177.0 43.3 %collective-permute-start.12 = (bf16[2,384,1024]{2,1,0:T(8,128)(2,1)}, bf16[2,384,1024]{2,1,0:T(8,128)(2,1)}, u32[]{:S(2)}, u32[]{:S(2)}) collective-permute-start(bf16[2,384,1024]{2,1,0:T(8,128)(2,1)} %pad_maximum_fusion.refs_8_), channel_id=1, source_target_pairs={{0,1},{1,0},{2,3},{3,2},{4,5},{5,4},{6,7},{7,6},{8,9},{9,8},{10,11... | collective-permute-start | bytes 4718600 | tf_op jit(solution)/shard_map/ppermute | solution.py:27
  177.8 43.9 %collective-permute-start.18 = (bf16[2,384,1024]{2,1,0:T(8,128)(2,1)}, bf16[2,384,1024]{2,1,0:T(8,128)(2,1)}, u32[]{:S(2)}, u32[]{:S(2)}) collective-permute-start(bf16[2,384,1024]{2,1,0:T(8,128)(2,1)} %pad_maximum_fusion.1.refs_12_), channel_id=1, source_target_pairs={{0,1},{1,0},{2,3},{3,2},{4,5},{5,4},{6,7},{7,6},{8,9},{9,8},{10,11... | collective-permute-start | bytes 4718600 | tf_op jit(solution)/shard_map/ppermute | solution.py:27
  178.3 46.6 %collective-permute-start.14 = (bf16[2,384,1024]{2,1,0:T(8,128)(2,1)}, bf16[2,384,1024]{2,1,0:T(8,128)(2,1)}, u32[]{:S(2)}, u32[]{:S(2)}) collective-permute-start(bf16[2,384,1024]{2,1,0:T(8,128)(2,1)} %collective-permute-done.13.refs_10_), channel_id=1, source_target_pairs={{0,1},{1,0},{2,3},{3,2},{4,5},{5,4},{6,7},{7,6},{8,9},{9,8},{10,11... | collective-permute-start | bytes 4718600 | tf_op jit(solution)/shard_map/ppermute | solution.py:27
  178.3 48.7 %collective-permute-start.20 = (bf16[2,384,1024]{2,1,0:T(8,128)(2,1)}, bf16[2,384,1024]{2,1,0:T(8,128)(2,1)}, u32[]{:S(2)}, u32[]{:S(2)}) collective-permute-start(bf16[2,384,1024]{2,1,0:T(8,128)(2,1)} %collective-permute-done.19.refs_14_), channel_id=1, source_target_pairs={{0,1},{1,0},{2,3},{3,2},{4,5},{5,4},{6,7},{7,6},{8,9},{9,8},{10,11... | collective-permute-start | bytes 4718600 | tf_op jit(solution)/shard_map/ppermute | solution.py:27
  220.2 60.8 %collective-permute-start.31 = (bf16[2,512,256]{2,1,0:T(8,128)(2,1)}, bf16[2,512,256]{2,1,0:T(8,128)(2,1)S(1)}, u32[]{:S(2)}, u32[]{:S(2)}) collective-permute-start(bf16[2,512,256]{2,1,0:T(8,128)(2,1)} %get-tuple-element.75), channel_id=1, source_target_pairs={{0,16},{4,20},{8,24},{12,28},{16,0},{20,4},{24,8},{28,12},{1,17},{... | collective-permute-start | bytes 1572872 | tf_op jit(solution)/shard_map/ppermute | solution.py:27
  221.7 71.4 %collective-permute-start.32 = (bf16[2,512,256]{2,1,0:T(8,128)(2,1)}, bf16[2,512,256]{2,1,0:T(8,128)(2,1)S(1)}, u32[]{:S(2)}, u32[]{:S(2)}) collective-permute-start(bf16[2,512,256]{2,1,0:T(8,128)(2,1)} %get-tuple-element.76), channel_id=1, source_target_pairs={{0,20},{4,16},{8,28},{12,24},{16,4},{20,0},{24,12},{28,8},{1,21},{... | collective-permute-start | bytes 1572872 | tf_op jit(solution)/shard_map/ppermute | solution.py:27
  224.9 68.3 %collective-permute-start.33 = (bf16[2,512,256]{2,1,0:T(8,128)(2,1)}, bf16[2,512,256]{2,1,0:T(8,128)(2,1)S(1)}, u32[]{:S(2)}, u32[]{:S(2)}) collective-permute-start(bf16[2,512,256]{2,1,0:T(8,128)(2,1)} %get-tuple-element.77), channel_id=1, source_target_pairs={{0,24},{4,28},{8,16},{12,20},{16,8},{20,12},{24,0},{28,4},{1,25},{... | collective-permute-start | bytes 1572872 | tf_op jit(solution)/shard_map/ppermute | solution.py:27
  227.0 66.2 %collective-permute-start.34 = (bf16[2,512,256]{2,1,0:T(8,128)(2,1)}, bf16[2,512,256]{2,1,0:T(8,128)(2,1)S(1)}, u32[]{:S(2)}, u32[]{:S(2)}) collective-permute-start(bf16[2,512,256]{2,1,0:T(8,128)(2,1)} %get-tuple-element.78), channel_id=1, source_target_pairs={{0,28},{4,24},{8,20},{12,16},{16,12},{20,8},{24,4},{28,0},{1,29},{... | collective-permute-start | bytes 1572872 | tf_op jit(solution)/shard_map/ppermute | solution.py:27
  302.9 42.2 %collective-permute-start.35 = (bf16[2,768,256]{2,1,0:T(8,128)(2,1)S(1)}, bf16[2,768,256]{2,1,0:T(8,128)(2,1)S(1)}, u32[]{:S(2)}, u32[]{:S(2)}) collective-permute-start(bf16[2,768,256]{2,1,0:T(8,128)(2,1)S(1)} %get-tuple-element.79), channel_id=1, source_target_pairs={{0,1},{1,0},{2,3},{3,2},{4,5},{5,4},{6,7},{7,6},{8,9},{9,8},{10,11... | collective-permute-start | bytes 2359304 | tf_op jit(solution)/shard_map/ppermute | solution.py:27
  325.5 61.0 %collective-permute-start.37 = (bf16[2,768,256]{2,1,0:T(8,128)(2,1)S(1)}, bf16[2,768,256]{2,1,0:T(8,128)(2,1)S(1)}, u32[]{:S(2)}, u32[]{:S(2)}) collective-permute-start(bf16[2,768,256]{2,1,0:T(8,128)(2,1)S(1)} %collective-permute-done.36), channel_id=1, source_target_pairs={{0,1},{1,0},{2,3},{3,2},{4,5},{5,4},{6,7},{7,6},{8,9},{9,8},{10,11... | collective-permute-start | bytes 2359304 | tf_op jit(solution)/shard_map/ppermute | solution.py:27
  333.4 41.2 %collective-permute-start.49 = (bf16[128,1024]{1,0:T(8,128)(2,1)S(1)}, bf16[128,1024]{1,0:T(8,128)(2,1)S(1)}, u32[]{:S(2)}, u32[]{:S(2)}) collective-permute-start(bf16[128,1024]{1,0:T(8,128)(2,1)S(1)} %get-tuple-element.93), channel_id=1, source_target_pairs={{0,20},{4,16},{8,28},{12,24},{16,4},{20,0},{24,12},{28,8},{1,21},{... | collective-permute-start | bytes 786440 | tf_op jit(solution)/shard_map/ppermute | solution.py:27
  345.1 41.5 %collective-permute-start.51 = (bf16[128,1024]{1,0:T(8,128)(2,1)S(1)}, bf16[128,1024]{1,0:T(8,128)(2,1)S(1)}, u32[]{:S(2)}, u32[]{:S(2)}) collective-permute-start(bf16[128,1024]{1,0:T(8,128)(2,1)S(1)} %get-tuple-element.95), channel_id=1, source_target_pairs={{0,28},{4,24},{8,20},{12,16},{16,12},{20,8},{24,4},{28,0},{1,29},{... | collective-permute-start | bytes 786440 | tf_op jit(solution)/shard_map/ppermute | solution.py:27
  363.1 45.0 %collective-permute-start.27 = (bf16[128,1024]{1,0:T(8,128)(2,1)S(1)}, bf16[128,1024]{1,0:T(8,128)(2,1)S(1)}, u32[]{:S(2)}, u32[]{:S(2)}) collective-permute-start(bf16[128,1024]{1,0:T(8,128)(2,1)S(1)} %get-tuple-element.70), channel_id=1, source_target_pairs={{0,28},{4,24},{8,20},{12,16},{16,12},{20,8},{24,4},{28,0},{1,29},{... | collective-permute-start | bytes 786440 | tf_op jit(solution)/shard_map/ppermute | solution.py:27
  376.2 44.5 %collective-permute-start.25 = (bf16[128,1024]{1,0:T(8,128)(2,1)S(1)}, bf16[128,1024]{1,0:T(8,128)(2,1)S(1)}, u32[]{:S(2)}, u32[]{:S(2)}) collective-permute-start(bf16[128,1024]{1,0:T(8,128)(2,1)S(1)} %get-tuple-element.68), channel_id=1, source_target_pairs={{0,20},{4,16},{8,28},{12,24},{16,4},{20,0},{24,12},{28,8},{1,21},{... | collective-permute-start | bytes 786440 | tf_op jit(solution)/shard_map/ppermute | solution.py:27
  445.1 59.6 %collective-permute-start.59 = (bf16[256,1024]{1,0:T(8,128)(2,1)}, bf16[256,1024]{1,0:T(8,128)(2,1)S(1)}, u32[]{:S(2)}, u32[]{:S(2)}) collective-permute-start(bf16[256,1024]{1,0:T(8,128)(2,1)} %get-tuple-element.107), channel_id=1, source_target_pairs={{0,1},{1,0},{2,3},{3,2},{4,5},{5,4},{6,7},{7,6},{8,9},{9,8},{10,11... | collective-permute-start | bytes 1572872 | tf_op jit(solution)/shard_map/ppermute | solution.py:27
  (65 other events, 1401.3 us)
